TPU v7x, 128 devices: a whole 4x4x4 slice. The times are simulated.
128 devices in a mesh: sp: 16 (over z, y), dp: 8 (over x, core).
Axes of the slice: x: 4, y: 4, z: 4, core: 2. Of those that a mesh axis runs over, the one named last changes fastest.
Arguments:
- tokens: bfloat16 [8, 4096, 2048], P('dp', 'sp'), may hold values from -6 to 6
- in_gain: float32 [2048], replicated, may hold values from 0.1 to 1.9
- w_query_down: bfloat16 [2048, 512], P('dp'), may hold values from -0.125 to 0.125
- w_latent_down: bfloat16 [2048, 256], P('dp'), may hold values from -0.125 to 0.125
- w_rope_key: bfloat16 [2048, 64], replicated, may hold values from -0.125 to 0.125
- query_latent_gain: float32 [512], replicated, may hold values from 0.1 to 1.9
- latent_gain: float32 [256], replicated, may hold values from 0.1 to 1.9
- w_query_up: bfloat16 [512, 3072], P('dp', 'sp'), may hold values from -0.25 to 0.25
- w_key_up: bfloat16 [256, 2048], P('dp', 'sp'), may hold values from -0.375 to 0.375
- w_value_up: bfloat16 [256, 2048], P('dp', 'sp'), may hold values from -0.375 to 0.375
- query_gain: float32 [192], replicated, may hold values from 0.5 to 14
- key_gain: float32 [192], replicated, may hold values from 0.5 to 14
- out_gain: float32 [2048], replicated, may hold values from 0.1 to 1.9
- w_out: bfloat16 [2048, 2048], P(('sp', 'dp')), may hold values from -0.125 to 0.125
Outputs:
- result: bfloat16 [8, 4096, 2048], P('dp', 'sp')
All inputs are finite; a program needn't handle non-finite values.
Results may differ from a plain program's by a relative error of at most 0.034.
The roundings to bfloat16 on the way count: a program that leaves them out, or rounds other values in their place, can miss the bound.
Values may be sent and summed in bfloat16 or wider, within the bound.
No kernel may reach another device: no remote copies, remote signals or barrier semaphores. Data moves between devices by JAX's collectives and lax.ppermute only.
A program may use at most 64 MiB of HBM per device.

v0:
```python
import jax
import jax.numpy as jnp
from jax import lax
from jax.sharding import PartitionSpec as P

HEADS = 16
EPS = 1e-06
THETA = 10000.0
NEG_BIG = -1e30


def in_one_piece(arrays, axis, dim, along):
    ends, at = ([], 0)
    for a in arrays[:-1]:
        at += a.shape[along]
        ends.append(at)
    both = jnp.concatenate(arrays, axis=along)
    return tuple(jnp.split(lax.all_gather(both, axis, axis=dim, tiled=True), ends, axis=along))


def joined_along(blocks, dim):
    dims = list(blocks.shape[1:])
    dims[dim] *= blocks.shape[0]
    return jnp.moveaxis(blocks, 0, dim).reshape(dims)


def sent_to_all(value, axis):
    copies = jnp.broadcast_to(value, (lax.axis_size(axis), *value.shape))
    return lax.all_to_all(copies, axis, split_axis=0, concat_axis=0, tiled=True)


def gathered_copies(value, axis, dim):
    return joined_along(sent_to_all(value, axis), dim)


def rms_scale(values, scaling):
    return values * lax.rsqrt(jnp.mean(values * values, axis=-1, keepdims=True) + EPS) * scaling


def rotate(tail_part, positions):
    half_width = tail_part.shape[-1] // 2
    frequency = THETA ** (-jnp.arange(half_width, dtype=jnp.float32) / half_width)
    angles = positions[:, None] * frequency[None, :]
    cosine = jnp.cos(angles)[:, None, :]
    sine = jnp.sin(angles)[:, None, :]
    first_half = tail_part[..., :half_width]
    second_half = tail_part[..., half_width:]
    return jnp.concatenate(
        [first_half * cosine - second_half * sine, second_half * cosine + first_half * sine],
        axis=-1,
    )


def finish_heads(joined, positions, scaling, rope_width):
    row_count = joined.shape[0]
    normal = rms_scale(joined, scaling)
    turned = rotate(normal[..., -rope_width:], positions)
    return (
        jnp.concatenate([normal[..., :-rope_width], turned], axis=-1)
        .astype(jnp.bfloat16)
        .reshape(row_count, -1)
    )


def make_queries(query_total, positions, scaling, head_count, rope_width):
    row_count = query_total.shape[0]
    return finish_heads(
        query_total.reshape(row_count, head_count, -1), positions, scaling, rope_width
    )


def make_keys(key_total, rope_key, positions, scaling, head_count):
    row_count = key_total.shape[0]
    rope_width = rope_key.shape[1]
    shaped = key_total.reshape(row_count, head_count, -1)
    shared = rope_key.astype(jnp.float32)[:, None, :]
    return finish_heads(jnp.concatenate([shaped, shared], axis=-1), positions, scaling, rope_width)


def single_fold(inputs, piece):
    return jnp.dot(inputs, piece, preferred_element_type=jnp.float32)


def double_fold(inputs, pieces):
    return (
        jnp.dot(inputs, pieces[0], preferred_element_type=jnp.float32),
        jnp.dot(inputs, pieces[1], preferred_element_type=jnp.float32),
    )


def attend(queries, keys, values, head_count):
    length = queries.shape[0]
    block_rows = min(512, length)
    query_blocks = queries.reshape(length // block_rows, block_rows, head_count, -1)
    key_heads = keys.reshape(length, head_count, -1)
    value_heads = values.reshape(length, head_count, -1)
    score_scale = key_heads.shape[-1] ** (-0.5)
    key_pos = jnp.arange(length)

    def one_block(block_args):
        query_block, block_index = block_args
        scores = (
            jnp.einsum("qhd,khd->hqk", query_block, key_heads, preferred_element_type=jnp.float32)
            * score_scale
        )
        query_pos = block_index * block_rows + jnp.arange(block_rows)
        allowed = key_pos[None, :] <= query_pos[:, None]
        scores = jnp.where(allowed[None], scores, NEG_BIG)
        weights = jax.nn.softmax(scores, axis=-1).astype(jnp.bfloat16)
        return jnp.einsum(
            "hqk,khd->qhd", weights, value_heads, preferred_element_type=jnp.float32
        ).astype(jnp.bfloat16)

    outcome = lax.map(one_block, (query_blocks, jnp.arange(length // block_rows)))
    return outcome.reshape(length, -1)


def per_device(
    tokens,
    in_gain,
    w_query_down,
    w_latent_down,
    w_rope_key,
    query_latent_gain,
    latent_gain,
    w_query_up,
    w_key_up,
    w_value_up,
    query_gain,
    key_gain,
    out_gain,
    w_out,
):
    seq_devices = lax.axis_size("sp")
    head_count = HEADS // seq_devices
    own_rows = tokens.shape[1]
    length = own_rows * seq_devices
    rope_width = w_rope_key.shape[1]
    local_rows = tokens.reshape(own_rows, tokens.shape[2])
    normed = rms_scale(local_rows.astype(jnp.float32), in_gain).astype(jnp.bfloat16)
    query_sum, latent_sum = double_fold(
        normed, in_one_piece((w_query_down, w_latent_down), "dp", 0, 1)
    )
    latent_q = rms_scale(query_sum, query_latent_gain).astype(jnp.bfloat16)
    latent_kv = rms_scale(latent_sum, latent_gain).astype(jnp.bfloat16)
    rope_key = jnp.dot(normed, w_rope_key, preferred_element_type=jnp.float32).astype(jnp.bfloat16)
    every_q, every_kv, every_rope = in_one_piece((latent_q, latent_kv, rope_key), "sp", 0, 1)
    positions = jnp.arange(length, dtype=jnp.float32)
    query_total = single_fold(every_q, gathered_copies(w_query_up, "dp", 0))
    key_total, value_total = double_fold(
        every_kv,
        (
            lax.all_gather(w_key_up, "dp", axis=0, tiled=True),
            lax.all_gather(w_value_up, "dp", axis=0, tiled=True),
        ),
    )
    queries = make_queries(query_total, positions, query_gain, head_count, rope_width)
    keys = make_keys(key_total, every_rope, positions, key_gain, head_count)
    values = value_total.astype(jnp.bfloat16)
    attended = attend(queries, keys, values, head_count)
    token_heads = lax.all_to_all(attended, "sp", split_axis=0, concat_axis=1, tiled=True)
    mixed = rms_scale(token_heads.astype(jnp.float32), out_gain).astype(jnp.bfloat16)
    projected = single_fold(mixed, lax.all_gather(w_out, ("sp", "dp"), axis=0, tiled=True))
    return projected.astype(jnp.bfloat16).reshape(1, own_rows, w_out.shape[1])


def solution(mesh):
    in_specs = (
        P("dp", "sp", None),
        P(),
        P("dp", None),
        P("dp", None),
        P(),
        P(),
        P(),
        P("dp", "sp"),
        P("dp", "sp"),
        P("dp", "sp"),
        P(),
        P(),
        P(),
        P(("sp", "dp"), None),
    )
    out_specs = P("dp", "sp", None)
    return jax.shard_map(
        per_device, mesh=mesh, in_specs=in_specs, out_specs=out_specs, check_vma=False
    )
```

profile of v0, /device:TPU:0, one launch (start us, length us, event | category | flops | bytes accessed | tf_op | source)
XLA Modules:
  0.0 225.6 jit_solution(16825096950358641469)
XLA Ops:
  6.5 1.9 pad_maximum_fusion.4
  8.5 1.5 fusion.17
  10.0 1.7 convolution_convert_fusion.2
  11.9 27.3 %all-gather.4.cloned.1.call-done = bf16[2048,768]{1,0:T(8,128)(2,1)} async-done(((bf16[256,768]{1,0:T(8,128)(2,1)}), bf16[2048,768]{1,0:T(8,128)(2,1)}) %all-gather.4.cloned.1.call-update) | async-done | bytes 3145744 | tf_op jit(solution)/shard_map/all_gather | solution.py:18
  39.2 2.4 %multiply_reduce_fusion.2 = (f32[256]{0:T(256)S(1)}, f32[256,512]{1,0:T(8,128)S(1)}) fusion(bf16[2048,768]{1,0:T(8,128)(2,1)} %all-gather.4.cloned.1.call-done, bf16[1,256,2048]{2,1,0:T(8,128)(2,1)S(1)} %copy-done.2, f32[2048]{0:T(1024)S(1)} %copy-done.11, f32[256]{0:T(256)S(1)} %add_rsqrt_fusion.5), kind=kOutput, calls=%fused_computation.61 | convolution fusion | flops 539229952 | bytes 3680256 | tf_op jit(solution)/shard_map/dot_general | solution.py:86
  41.7 1.9 multiply_reduce_fusion.3
  44.0 0.8 pad_maximum_fusion.3
  44.8 0.7 broadcast_in_dim.11
  45.6 4.0 %all-to-all-start = ((bf16[8,64,192]{2,1,0:T(8,128)(2,1)}), bf16[8,64,192]{2,1,0:T(8,128)(2,1)}, u32[]{:S(2)}, u32[]{:S(2)}) async-start(bf16[8,64,192]{2,1,0:T(8,128)(2,1)} %broadcast_in_dim.11), calls=%async_computation | async-start | bytes 524288 | tf_op jit(solution)/shard_map/all_to_all | solution.py:29
  49.7 0.7 all-gather.8.cloned.1.call-update
  50.4 13.8 %all_gather.17 = bf16[256,128]{1,0:T(8,128)(2,1)S(1)} all-gather(bf16[32,128]{1,0:T(8,128)(2,1)S(1)} %copy-done.5), channel_id=1, replica_groups=mesh['sp'=16,'dp'=8] {'dp'}, dimensions={0}, use_global_device_ids=true | all-gather | bytes 73728 | tf_op jit(solution)/shard_map/all_gather | solution.py:153
  64.2 12.9 %all_gather.18 = bf16[256,128]{1,0:T(8,128)(2,1)S(1)} all-gather(bf16[32,128]{1,0:T(8,128)(2,1)S(1)} %copy-done.6), channel_id=1, replica_groups=mesh['sp'=16,'dp'=8] {'dp'}, dimensions={0}, use_global_device_ids=true | all-gather | bytes 73728 | tf_op jit(solution)/shard_map/all_gather | solution.py:154
  77.1 34.1 %all-gather.6.cloned.1.call-done = bf16[4096,832]{1,0:T(8,128)(2,1)} async-done(((bf16[256,832]{1,0:T(8,128)(2,1)}), bf16[4096,832]{1,0:T(8,128)(2,1)}) %all-gather.6.cloned.1.call-update) | async-done | bytes 6815760 | tf_op jit(solution)/shard_map/all_gather | solution.py:18
  111.2 1.4 fusion.26
  113.1 2.4 %convolution_bitcast_fusion = f32[4096,1,128]{0,2,1:T(8,128)S(1)} fusion(bf16[256,128]{1,0:T(8,128)(2,1)S(1)} %all_gather.17, bf16[4096,832]{1,0:T(8,128)(2,1)} %all-gather.6.cloned.1.call-done), kind=kOutput, calls=%fused_computation.16 | convolution fusion | flops 268435456 | bytes 4259840 | tf_op jit(solution)/shard_map/dot_general | solution.py:86
  115.8 3.8 %multiply_reduce_fusion.1 = (f32[4096]{0:T(1024)S(1)}, f32[4096,192]{0,1:T(8,128)S(1)}) fusion(bf16[512,192]{1,0:T(8,128)(2,1)} %bitcast.2, bf16[4096,832]{1,0:T(8,128)(2,1)} %all-gather.6.cloned.1.call-done), kind=kOutput, calls=%fused_computation.25 | convolution fusion | flops 806875136 | bytes 7618560 | tf_op jit(solution)/shard_map/dot_general | solution.py:81
  120.9 2.5 %subtract_convert_fusion = (bf16[4096,1,32]{0,2,1:T(8,128)(2,1)S(1)}, bf16[4096,1,32]{0,2,1:T(8,128)(2,1)S(1)}, bf16[4096,1,32]{0,2,1:T(8,128)(2,1)S(1)}, bf16[4096,1,32]{0,2,1:T(8,128)(2,1)S(1)}) fusion(f32[4096,1,192]{0,2,1:T(8,128)S(1)} %multiply_multiply_fusion, f32[32]{0:T(128)S(1)} %multiply_power_fusion, f32[4096,1,192]{0,2,1:T(8,128)S(1)} %multiply_bitcast_fusion), kind=kLoop, calls=%fused_computation.54 | loop fusion | flops 2228224 | bytes 3145856 | tf_op jit(solution)/shard_map/convert.5
  123.9 3.3 %fusion.12 = bf16[4096,1,128]{2,0,1:T(8,128)(2,1)} fusion(bf16[256,128]{1,0:T(8,128)(2,1)S(1)} %all_gather.18, bf16[4096,832]{1,0:T(8,128)(2,1)} %all-gather.6.cloned.1.call-done), kind=kOutput, calls=%fused_computation.18 | convolution fusion | flops 268959744 | bytes 3211264 | tf_op jit(solution)/shard_map/dot_general | solution.py:87
  127.2 58.7 %while.11 = (s32[]{:T(128)}, bf16[8,512,1,128]{3,1,2,0:T(8,128)(2,1)}, s32[8]{0:T(128)S(1)}, bf16[8,512,1,192]{1,3,2,0:T(8,128)(2,1)S(1)}, bf16[4096,1,192]{0,2,...) while((s32[]{:T(128)}, bf16[8,512,1,128]{3,1,2,0:T(8,128)(2,1)}, ...), condition=%wide.region_8.9_spmd.clone, body=%wide.region_5.8_spmd.clone.sunk | while | flops 1361116672 | bytes 32324240 | solution.py:114
  127.2 0.6 dynamic_slice.19
  128.5 1.9 fusion.46
  130.4 1.3 fusion.47
  131.7 2.8 %fusion.48 = bf16[8,512,1,128]{3,1,2,0:T(8,128)(2,1)} fusion(bf16[8,512,1,128]{3,1,2,0:T(8,128)(2,1)} %get-tuple-element.141, s32[]{:T(128)} %get-tuple-element.140, f32[512,4096]{1,0:T(8,128)S(1)} %get-tuple-element.130, f32[512]{0:T(512)S(1)} %fusion.47, f32[512]{0:T(512)S(1)} %get-tuple-element.131, bf16[4096,1,128]{2,0,1:T(8,128)(2,1)S(1)} %copy-done.1), kind=kOutput, calls=%fused_computation.10.clone.1 | convolution fusion | flops 543227904 | bytes 9572864 | tf_op jit(solution)/shard_map/while/body/eval_jaxpr/hqk,khd->qhd/dot_general | solution.py:110
  135.8 2.0 fusion.46
  137.8 1.3 fusion.47
  139.0 2.8 %fusion.48 = bf16[8,512,1,128]{3,1,2,0:T(8,128)(2,1)} fusion(bf16[8,512,1,128]{3,1,2,0:T(8,128)(2,1)} %get-tuple-element.141, s32[]{:T(128)} %get-tuple-element.140, f32[512,4096]{1,0:T(8,128)S(1)} %get-tuple-element.130, f32[512]{0:T(512)S(1)} %fusion.47, f32[512]{0:T(512)S(1)} %get-tuple-element.131, bf16[4096,1,128]{2,0,1:T(8,128)(2,1)S(1)} %copy-done.1), kind=kOutput, calls=%fused_computation.10.clone.1 | convolution fusion | flops 543227904 | bytes 9572864 | tf_op jit(solution)/shard_map/while/body/eval_jaxpr/hqk,khd->qhd/dot_general | solution.py:110
  143.1 2.0 fusion.46
  145.1 1.3 fusion.47
  146.4 2.8 %fusion.48 = bf16[8,512,1,128]{3,1,2,0:T(8,128)(2,1)} fusion(bf16[8,512,1,128]{3,1,2,0:T(8,128)(2,1)} %get-tuple-element.141, s32[]{:T(128)} %get-tuple-element.140, f32[512,4096]{1,0:T(8,128)S(1)} %get-tuple-element.130, f32[512]{0:T(512)S(1)} %fusion.47, f32[512]{0:T(512)S(1)} %get-tuple-element.131, bf16[4096,1,128]{2,0,1:T(8,128)(2,1)S(1)} %copy-done.1), kind=kOutput, calls=%fused_computation.10.clone.1 | convolution fusion | flops 543227904 | bytes 9572864 | tf_op jit(solution)/shard_map/while/body/eval_jaxpr/hqk,khd->qhd/dot_general | solution.py:110
  150.5 2.0 fusion.46
  152.4 1.3 fusion.47
  153.7 2.8 %fusion.48 = bf16[8,512,1,128]{3,1,2,0:T(8,128)(2,1)} fusion(bf16[8,512,1,128]{3,1,2,0:T(8,128)(2,1)} %get-tuple-element.141, s32[]{:T(128)} %get-tuple-element.140, f32[512,4096]{1,0:T(8,128)S(1)} %get-tuple-element.130, f32[512]{0:T(512)S(1)} %fusion.47, f32[512]{0:T(512)S(1)} %get-tuple-element.131, bf16[4096,1,128]{2,0,1:T(8,128)(2,1)S(1)} %copy-done.1), kind=kOutput, calls=%fused_computation.10.clone.1 | convolution fusion | flops 543227904 | bytes 9572864 | tf_op jit(solution)/shard_map/while/body/eval_jaxpr/hqk,khd->qhd/dot_general | solution.py:110
  157.8 2.0 fusion.46
  159.8 1.3 fusion.47
  161.0 2.8 %fusion.48 = bf16[8,512,1,128]{3,1,2,0:T(8,128)(2,1)} fusion(bf16[8,512,1,128]{3,1,2,0:T(8,128)(2,1)} %get-tuple-element.141, s32[]{:T(128)} %get-tuple-element.140, f32[512,4096]{1,0:T(8,128)S(1)} %get-tuple-element.130, f32[512]{0:T(512)S(1)} %fusion.47, f32[512]{0:T(512)S(1)} %get-tuple-element.131, bf16[4096,1,128]{2,0,1:T(8,128)(2,1)S(1)} %copy-done.1), kind=kOutput, calls=%fused_computation.10.clone.1 | convolution fusion | flops 543227904 | bytes 9572864 | tf_op jit(solution)/shard_map/while/body/eval_jaxpr/hqk,khd->qhd/dot_general | solution.py:110
  165.1 2.0 fusion.46
  167.1 1.3 fusion.47
  168.4 2.8 %fusion.48 = bf16[8,512,1,128]{3,1,2,0:T(8,128)(2,1)} fusion(bf16[8,512,1,128]{3,1,2,0:T(8,128)(2,1)} %get-tuple-element.141, s32[]{:T(128)} %get-tuple-element.140, f32[512,4096]{1,0:T(8,128)S(1)} %get-tuple-element.130, f32[512]{0:T(512)S(1)} %fusion.47, f32[512]{0:T(512)S(1)} %get-tuple-element.131, bf16[4096,1,128]{2,0,1:T(8,128)(2,1)S(1)} %copy-done.1), kind=kOutput, calls=%fused_computation.10.clone.1 | convolution fusion | flops 543227904 | bytes 9572864 | tf_op jit(solution)/shard_map/while/body/eval_jaxpr/hqk,khd->qhd/dot_general | solution.py:110
  172.5 2.0 fusion.46
  174.4 1.3 fusion.47
  175.8 2.8 %fusion.48 = bf16[8,512,1,128]{3,1,2,0:T(8,128)(2,1)} fusion(bf16[8,512,1,128]{3,1,2,0:T(8,128)(2,1)} %get-tuple-element.141, s32[]{:T(128)} %get-tuple-element.140, f32[512,4096]{1,0:T(8,128)S(1)} %get-tuple-element.130, f32[512]{0:T(512)S(1)} %fusion.47, f32[512]{0:T(512)S(1)} %get-tuple-element.131, bf16[4096,1,128]{2,0,1:T(8,128)(2,1)S(1)} %copy-done.1), kind=kOutput, calls=%fused_computation.10.clone.1 | convolution fusion | flops 543227904 | bytes 9572864 | tf_op jit(solution)/shard_map/while/body/eval_jaxpr/hqk,khd->qhd/dot_general | solution.py:110
  179.9 1.9 fusion.46
  181.8 1.3 fusion.47
  183.1 2.8 %fusion.48 = bf16[8,512,1,128]{3,1,2,0:T(8,128)(2,1)} fusion(bf16[8,512,1,128]{3,1,2,0:T(8,128)(2,1)} %get-tuple-element.141, s32[]{:T(128)} %get-tuple-element.140, f32[512,4096]{1,0:T(8,128)S(1)} %get-tuple-element.130, f32[512]{0:T(512)S(1)} %fusion.47, f32[512]{0:T(512)S(1)} %get-tuple-element.131, bf16[4096,1,128]{2,0,1:T(8,128)(2,1)S(1)} %copy-done.1), kind=kOutput, calls=%fused_computation.10.clone.1 | convolution fusion | flops 543227904 | bytes 9572864 | tf_op jit(solution)/shard_map/while/body/eval_jaxpr/hqk,khd->qhd/dot_general | solution.py:110
  185.9 22.2 %all_to_all.18 = bf16[16,256,128]{2,1,0:T(8,128)(2,1)S(1)} all-to-all(bf16[16,256,128]{2,1,0:T(8,128)(2,1)} %bitcast.7), channel_id=1, replica_groups=mesh['sp'=16,'dp'=8] {'sp'}, dimensions={0} | all-to-all | bytes 2097152 | tf_op jit(solution)/shard_map/all_to_all | solution.py:161
  208.2 1.6 convert_bitcast_fusion
  209.7 1.9 copy.42
  212.4 6.7 %fusion.15 = bf16[1,256,2048]{2,1,0:T(8,128)(2,1)} fusion(bf16[256,2048]{0,1:T(8,128)(2,1)S(1)} %fusion.23, bf16[2048,2048]{1,0:T(8,128)(2,1)} %all-gather.8.cloned.1.call-done), kind=kOutput, calls=%fused_computation.31 | convolution fusion | flops 2148007936 | bytes 10485760 | tf_op jit(solution)/shard_map/dot_general | solution.py:81
  (85 shorter events, 8.3 us)
Async XLA Ops:
  6.5 3.5 %copy-start = (bf16[2048,64]{0,1:T(8,128)(2,1)S(1)}, bf16[2048,64]{0,1:T(8,128)(2,1)}, u32[]{:S(2)}) copy-start(bf16[2048,64]{0,1:T(8,128)(2,1)} %param.20) | copy-start | bytes 786436
  6.5 32.7 %copy-start.2 = (bf16[1,256,2048]{2,1,0:T(8,128)(2,1)S(1)}, bf16[1,256,2048]{2,1,0:T(8,128)(2,1)}, u32[]{:S(2)}) copy-start(bf16[1,256,2048]{2,1,0:T(8,128)(2,1)} %param.16) | copy-start | bytes 3145732
  6.5 32.7 %copy-start.11 = (f32[2048]{0:T(1024)S(1)}, f32[2048]{0:T(1024)}, u32[]{:S(2)}) copy-start(f32[2048]{0:T(1024)} %param.17) | copy-start | bytes 24580
  6.5 32.7 %all-gather.4.cloned.1.call-start = ((), (), s32[]{:S(2)}) async-start(), calls=%async_computation.2 | async-start | bytes 3538944 | tf_op jit(solution)/shard_map/all_gather | solution.py:18
  8.5 102.7 %all-gather.6.cloned.1.call-start = ((), (), s32[]{:S(2)}) async-start(), calls=%async_computation.3 | async-start | bytes 7798784 | tf_op jit(solution)/shard_map/all_gather | solution.py:18
  41.6 2.1 copy-start.7
  41.6 2.2 copy-start.8
  41.7 3.2 %copy-start.3 = (bf16[64,192]{1,0:T(8,128)(2,1)S(1)}, bf16[64,192]{1,0:T(8,128)(2,1)}, u32[]{:S(2)}) copy-start(bf16[64,192]{1,0:T(8,128)(2,1)} %param.23) | copy-start | bytes 73732
  41.7 8.7 %copy-start.5 = (bf16[32,128]{1,0:T(8,128)(2,1)S(1)}, bf16[32,128]{1,0:T(8,128)(2,1)}, u32[]{:S(2)}) copy-start(bf16[32,128]{1,0:T(8,128)(2,1)} %param.24) | copy-start | bytes 24580
  41.7 22.5 %copy-start.6 = (bf16[32,128]{1,0:T(8,128)(2,1)S(1)}, bf16[32,128]{1,0:T(8,128)(2,1)}, u32[]{:S(2)}) copy-start(bf16[32,128]{1,0:T(8,128)(2,1)} %param.25) | copy-start | bytes 24580
  45.6 70.2 %all-to-all-start = ((bf16[8,64,192]{2,1,0:T(8,128)(2,1)}), bf16[8,64,192]{2,1,0:T(8,128)(2,1)}, u32[]{:S(2)}, u32[]{:S(2)}) async-start(bf16[8,64,192]{2,1,0:T(8,128)(2,1)} %broadcast_in_dim.11), calls=%async_computation | async-start | bytes 524288 | tf_op jit(solution)/shard_map/all_to_all | solution.py:29
  49.6 162.7 %all-gather.8.cloned.1.call-start = ((), (), s32[]{:S(2)}) async-start(), calls=%async_computation.4 | async-start | bytes 8454144 | tf_op jit(solution)/shard_map/all_gather | solution.py:163
  115.8 3.8 %copy-start.9 = (f32[192]{0:T(256)S(1)}, f32[192]{0:T(256)}, u32[]{:S(2)}) copy-start(f32[192]{0:T(256)} %param.27) | copy-start | bytes 2308
  119.6 0.7 copy-start.10
  130.4 1.3 copy-start.1
  137.7 1.3 copy-start.1
  145.1 1.3 copy-start.1
  152.4 1.3 copy-start.1
  159.8 1.3 copy-start.1
  167.1 1.3 copy-start.1
  174.4 1.4 copy-start.1
  181.8 1.3 copy-start.1
  209.7 2.2 copy-start.4
Sparse Core Ops, SparseCore 0:
  9.0 30.1 all-gather.3
  44.9 66.1 all-gather.5
  114.2 69.2 all-gather.7
where the time goes:
time: 226 us
  waiting for transfers between devices  62.1 us (27%)
  matrix products  60.5 us (27%)
  blocking collectives  48.9 us (22%)
  other arithmetic  22.3 us (10%)
  between operations  13.4 us (6%)
  local copies, waits for them, and re-layouts  8.96 us (4%)
  loops' own time  5.21 us (2%)
  starting transfers between devices  4.13 us (2%)
    all_gather x2, waiting for transfers between devices, in_one_piece(): lax.all_gather(both, axis, axis=dim, tiled=True)  61.4 us
    dot_general x8, matrix products, one_block(): jnp.einsum('hqk,khd->qhd', weights, value_heads, preferred_element_type=j...  22.6 us
    all_to_all x1, blocking collectives, per_device(): lax.all_to_all(attended, 'sp', split_axis=0, concat_axis=1, tiled=True)  22.2 us
    dot_general x8, matrix products, one_block(): jnp.einsum('qhd,khd->hqk', query_block, key_heads, preferred_element_type...  15.7 us
    all_gather x1, blocking collectives, per_device(): lax.all_gather(w_key_up, 'dp', axis=0, tiled=True)  13.8 us
    all_gather x1, blocking collectives, per_device(): lax.all_gather(w_value_up, 'dp', axis=0, tiled=True)  12.9 us
    dot_general x2, matrix products, single_fold(): return jnp.dot(inputs, piece, preferred_element_type=jnp.float32)  10.5 us
    reduce_sum x8, other arithmetic, one_block(): weights = jax.nn.softmax(scores, axis=-1).astype(jnp.bfloat16)  10.2 us
  transfers between devices with their start and end apart: 4, of which 2 were waited for; matrix products, arithmetic and copies ran while one was open for 34% of the time, Pallas kernels for 0%

commit v1 on v0

--- a/solution.py
+++ b/solution.py
@@ -150,7 +150,9 @@
     key_total, value_total = double_fold(
         every_kv,
         (
-            lax.all_gather(w_key_up, "dp", axis=0, tiled=True),
+            jnp.concatenate(
+                lax.all_to_all(jnp.stack([w_key_up] * lax.axis_size("dp")), "dp", 0, 0), axis=0
+            ),
             lax.all_gather(w_value_up, "dp", axis=0, tiled=True),
         ),
     )

time: 226 us -> 238 us (1.053)
  waiting for transfers between devices: 62.1 us -> 81 us
  blocking collectives: 48.9 us -> 35.3 us
  starting transfers between devices: 4.13 us -> 7.69 us
    all_gather x2, waiting for transfers between devices: 61.4 us -> 75.4 us  [in_one_piece(): lax.all_gather(both, axis, axis=dim, tiled=True)]
    all_gather x1 -> x0, blocking collectives: 13.8 us -> none  [per_device(): lax.all_gather(w_key_up, 'dp', axis=0, tiled=True)]
    all_to_all x1, waiting for transfers between devices: 0.01 us -> 4.92 us  [sent_to_all(): return lax.all_to_all(copies, axis, split_axis=0, concat_axis=0, tiled=True)]
    all_to_all x0 -> x1, starting transfers between devices: none -> 3.35 us  [per_device(): lax.all_to_all(jnp.stack([w_key_up] * lax.axis_size('dp')), 'dp', 0, 0)]
  transfers between devices with their start and end apart: 4 -> 5, of which waited for: 2 -> 3; matrix products, arithmetic and copies ran while one was open for 34% -> 33% of each run, Pallas kernels for 0% -> 0%
where the time goes in v1:
time: 238 us; the launch traced here: 237 us
  waiting for transfers between devices  81 us (34%)
  matrix products  60.4 us (25%)
  blocking collectives  35.3 us (15%)
  other arithmetic  22.3 us (9%)
  between operations  13.4 us (6%)
  local copies, waits for them, and re-layouts  10.9 us (5%)
  starting transfers between devices  7.69 us (3%)
  loops' own time  5.54 us (2%)
    all_gather x2, waiting for transfers between devices, in_one_piece(): lax.all_gather(both, axis, axis=dim, tiled=True)  75.4 us
    dot_general x8, matrix products, one_block(): jnp.einsum('hqk,khd->qhd', weights, value_heads, preferred_element_type=j...  22.6 us
    all_to_all x1, blocking collectives, per_device(): lax.all_to_all(attended, 'sp', split_axis=0, concat_axis=1, tiled=True)  21.8 us
    dot_general x8, matrix products, one_block(): jnp.einsum('qhd,khd->hqk', query_block, key_heads, preferred_element_type...  15.7 us
    all_gather x1, blocking collectives, per_device(): lax.all_gather(w_value_up, 'dp', axis=0, tiled=True)  13.5 us
    dot_general x2, matrix products, single_fold(): return jnp.dot(inputs, piece, preferred_element_type=jnp.float32)  10.5 us
    reduce_sum x8, other arithmetic, one_block(): weights = jax.nn.softmax(scores, axis=-1).astype(jnp.bfloat16)  10.2 us
    another operation x1, loops' own time, attend(): lax.map(one_block, (query_blocks, jnp.arange(length // block_rows)))  5.54 us
  transfers between devices with their start and end apart: 5, of which 3 were waited for; matrix products, arithmetic and copies ran while one was open for 33% of the time, Pallas kernels for 0%

profile of v1, /device:TPU:0, one launch (start us, length us, event | category | flops | bytes accessed | tf_op | source)
XLA Modules:
  0.0 236.6 jit_solution(13221884968214474306)
XLA Ops:
  6.5 1.9 pad_maximum_fusion.4
  8.5 1.5 fusion.17
  10.0 1.7 convolution_convert_fusion.2
  11.9 27.3 %all-gather.4.cloned.1.call-done = bf16[2048,768]{1,0:T(8,128)(2,1)} async-done(((bf16[256,768]{1,0:T(8,128)(2,1)}), bf16[2048,768]{1,0:T(8,128)(2,1)}) %all-gather.4.cloned.1.call-update) | async-done | bytes 3145744 | tf_op jit(solution)/shard_map/all_gather | solution.py:18
  39.2 2.4 %multiply_reduce_fusion.2 = (f32[256]{0:T(256)S(1)}, f32[256,512]{1,0:T(8,128)S(1)}) fusion(bf16[2048,768]{1,0:T(8,128)(2,1)} %all-gather.4.cloned.1.call-done, bf16[1,256,2048]{2,1,0:T(8,128)(2,1)S(1)} %copy-done.2, f32[2048]{0:T(1024)S(1)} %copy-done.10, f32[256]{0:T(256)S(1)} %add_rsqrt_fusion.5), kind=kOutput, calls=%fused_computation.61 | convolution fusion | flops 539229952 | bytes 3680256 | tf_op jit(solution)/shard_map/dot_general | solution.py:86
  41.7 1.9 multiply_reduce_fusion.3
  44.0 0.8 pad_maximum_fusion.3
  45.5 3.3 %all-to-all-start.1 = ((bf16[8,32,128]{2,1,0:T(8,128)(2,1)}), bf16[8,32,128]{2,1,0:T(8,128)(2,1)S(1)}, u32[]{:S(2)}, u32[]{:S(2)}) async-start(bf16[8,32,128]{2,1,0:T(8,128)(2,1)} %stack.2), calls=%async_computation.1 | async-start | bytes 131072 | tf_op jit(solution)/shard_map/all_to_all | solution.py:154
  48.9 0.7 all-gather.8.cloned.1.call-update
  49.6 13.5 %all_gather.14 = bf16[256,128]{1,0:T(8,128)(2,1)S(1)} all-gather(bf16[32,128]{1,0:T(8,128)(2,1)S(1)} %copy-done.5), channel_id=1, replica_groups=mesh['sp'=16,'dp'=8] {'dp'}, dimensions={0}, use_global_device_ids=true | all-gather | bytes 73728 | tf_op jit(solution)/shard_map/all_gather | solution.py:156
  63.1 48.1 %all-gather.6.cloned.1.call-done = bf16[4096,832]{1,0:T(8,128)(2,1)} async-done(((bf16[256,832]{1,0:T(8,128)(2,1)}), bf16[4096,832]{1,0:T(8,128)(2,1)}) %all-gather.6.cloned.1.call-update) | async-done | bytes 6815760 | tf_op jit(solution)/shard_map/all_gather | solution.py:18
  111.2 1.4 fusion.26
  113.1 1.5 broadcast_in_dim.11
  114.6 4.3 %all-to-all-start = ((bf16[8,64,192]{2,1,0:T(8,128)(2,1)}), bf16[8,64,192]{2,1,0:T(8,128)(2,1)}, u32[]{:S(2)}, u32[]{:S(2)}) async-start(bf16[8,64,192]{2,1,0:T(8,128)(2,1)} %broadcast_in_dim.11), calls=%async_computation | async-start | bytes 524288 | tf_op jit(solution)/shard_map/all_to_all | solution.py:29
  118.9 2.4 %convolution_bitcast_fusion = f32[4096,1,128]{0,2,1:T(8,128)S(1)} fusion(bf16[256,128]{1,0:T(8,128)(2,1)S(1)} %bitcast.89, bf16[4096,832]{1,0:T(8,128)(2,1)} %all-gather.6.cloned.1.call-done), kind=kOutput, calls=%fused_computation.16 | convolution fusion | flops 268435456 | bytes 4259840 | tf_op jit(solution)/shard_map/dot_general | solution.py:86
  121.6 4.9 %all-to-all-done = bf16[8,64,192]{2,1,0:T(8,128)(2,1)} async-done(((bf16[8,64,192]{2,1,0:T(8,128)(2,1)}), bf16[8,64,192]{2,1,0:T(8,128)(2,1)}, u32[]{:S(2)}, u32[]{:S(2)}) %all-to-all-start) | async-done | bytes 196640 | tf_op jit(solution)/shard_map/all_to_all | solution.py:29
  126.5 3.8 %multiply_reduce_fusion.1 = (f32[4096]{0:T(1024)S(1)}, f32[4096,192]{0,1:T(8,128)S(1)}) fusion(bf16[512,192]{1,0:T(8,128)(2,1)} %bitcast.2, bf16[4096,832]{1,0:T(8,128)(2,1)} %all-gather.6.cloned.1.call-done), kind=kOutput, calls=%fused_computation.25 | convolution fusion | flops 806875136 | bytes 7618560 | tf_op jit(solution)/shard_map/dot_general | solution.py:81
  131.6 2.5 %subtract_convert_fusion = (bf16[4096,1,32]{0,2,1:T(8,128)(2,1)S(1)}, bf16[4096,1,32]{0,2,1:T(8,128)(2,1)S(1)}, bf16[4096,1,32]{0,2,1:T(8,128)(2,1)S(1)}, bf16[4096,1,32]{0,2,1:T(8,128)(2,1)S(1)}) fusion(f32[4096,1,192]{0,2,1:T(8,128)S(1)} %multiply_multiply_fusion, f32[32]{0:T(128)S(1)} %multiply_power_fusion, f32[4096,1,192]{0,2,1:T(8,128)S(1)} %multiply_bitcast_fusion), kind=kLoop, calls=%fused_computation.54 | loop fusion | flops 2228224 | bytes 3145856 | tf_op jit(solution)/shard_map/convert.5
  134.5 3.3 %fusion.12 = bf16[4096,1,128]{2,0,1:T(8,128)(2,1)} fusion(bf16[256,128]{1,0:T(8,128)(2,1)S(1)} %all_gather.14, bf16[4096,832]{1,0:T(8,128)(2,1)} %all-gather.6.cloned.1.call-done), kind=kOutput, calls=%fused_computation.18 | convolution fusion | flops 268959744 | bytes 3211264 | tf_op jit(solution)/shard_map/dot_general | solution.py:87
  137.8 59.6 %while.11 = (s32[]{:T(128)}, bf16[8,512,1,128]{3,1,2,0:T(8,128)(2,1)}, s32[8]{0:T(128)S(1)}, bf16[8,512,1,192]{1,3,2,0:T(8,128)(2,1)S(1)}, bf16[4096,1,192]{0,2,...) while((s32[]{:T(128)}, bf16[8,512,1,128]{3,1,2,0:T(8,128)(2,1)}, ...), condition=%wide.region_8.9_spmd.clone, body=%wide.region_5.8_spmd.clone.sunk | while | flops 1361116672 | bytes 32324240 | solution.py:114
  139.2 2.0 fusion.46
  141.1 1.3 fusion.47
  142.4 2.8 %fusion.48 = bf16[8,512,1,128]{3,1,2,0:T(8,128)(2,1)} fusion(bf16[8,512,1,128]{3,1,2,0:T(8,128)(2,1)} %get-tuple-element.141, s32[]{:T(128)} %get-tuple-element.140, f32[512,4096]{1,0:T(8,128)S(1)} %get-tuple-element.130, f32[512]{0:T(512)S(1)} %fusion.47, f32[512]{0:T(512)S(1)} %get-tuple-element.131, bf16[4096,1,128]{2,0,1:T(8,128)(2,1)S(1)} %copy-done.1), kind=kOutput, calls=%fused_computation.10.clone.1 | convolution fusion | flops 543227904 | bytes 9572864 | tf_op jit(solution)/shard_map/while/body/eval_jaxpr/hqk,khd->qhd/dot_general | solution.py:110
  146.6 2.0 fusion.46
  148.5 1.3 fusion.47
  149.8 2.8 %fusion.48 = bf16[8,512,1,128]{3,1,2,0:T(8,128)(2,1)} fusion(bf16[8,512,1,128]{3,1,2,0:T(8,128)(2,1)} %get-tuple-element.141, s32[]{:T(128)} %get-tuple-element.140, f32[512,4096]{1,0:T(8,128)S(1)} %get-tuple-element.130, f32[512]{0:T(512)S(1)} %fusion.47, f32[512]{0:T(512)S(1)} %get-tuple-element.131, bf16[4096,1,128]{2,0,1:T(8,128)(2,1)S(1)} %copy-done.1), kind=kOutput, calls=%fused_computation.10.clone.1 | convolution fusion | flops 543227904 | bytes 9572864 | tf_op jit(solution)/shard_map/while/body/eval_jaxpr/hqk,khd->qhd/dot_general | solution.py:110
  154.0 2.0 fusion.46
  155.9 1.3 fusion.47
  157.2 2.8 %fusion.48 = bf16[8,512,1,128]{3,1,2,0:T(8,128)(2,1)} fusion(bf16[8,512,1,128]{3,1,2,0:T(8,128)(2,1)} %get-tuple-element.141, s32[]{:T(128)} %get-tuple-element.140, f32[512,4096]{1,0:T(8,128)S(1)} %get-tuple-element.130, f32[512]{0:T(512)S(1)} %fusion.47, f32[512]{0:T(512)S(1)} %get-tuple-element.131, bf16[4096,1,128]{2,0,1:T(8,128)(2,1)S(1)} %copy-done.1), kind=kOutput, calls=%fused_computation.10.clone.1 | convolution fusion | flops 543227904 | bytes 9572864 | tf_op jit(solution)/shard_map/while/body/eval_jaxpr/hqk,khd->qhd/dot_general | solution.py:110
  161.4 2.0 fusion.46
  163.3 1.3 fusion.47
  164.9 2.8 %fusion.48 = bf16[8,512,1,128]{3,1,2,0:T(8,128)(2,1)} fusion(bf16[8,512,1,128]{3,1,2,0:T(8,128)(2,1)} %get-tuple-element.141, s32[]{:T(128)} %get-tuple-element.140, f32[512,4096]{1,0:T(8,128)S(1)} %get-tuple-element.130, f32[512]{0:T(512)S(1)} %fusion.47, f32[512]{0:T(512)S(1)} %get-tuple-element.131, bf16[4096,1,128]{2,0,1:T(8,128)(2,1)S(1)} %copy-done.1), kind=kOutput, calls=%fused_computation.10.clone.1 | convolution fusion | flops 543227904 | bytes 9572864 | tf_op jit(solution)/shard_map/while/body/eval_jaxpr/hqk,khd->qhd/dot_general | solution.py:110
  169.0 2.0 fusion.46
  171.0 1.3 fusion.47
  172.4 2.8 %fusion.48 = bf16[8,512,1,128]{3,1,2,0:T(8,128)(2,1)} fusion(bf16[8,512,1,128]{3,1,2,0:T(8,128)(2,1)} %get-tuple-element.141, s32[]{:T(128)} %get-tuple-element.140, f32[512,4096]{1,0:T(8,128)S(1)} %get-tuple-element.130, f32[512]{0:T(512)S(1)} %fusion.47, f32[512]{0:T(512)S(1)} %get-tuple-element.131, bf16[4096,1,128]{2,0,1:T(8,128)(2,1)S(1)} %copy-done.1), kind=kOutput, calls=%fused_computation.10.clone.1 | convolution fusion | flops 543227904 | bytes 9572864 | tf_op jit(solution)/shard_map/while/body/eval_jaxpr/hqk,khd->qhd/dot_general | solution.py:110
  176.5 2.0 fusion.46
  178.5 1.3 fusion.47
  179.8 2.8 %fusion.48 = bf16[8,512,1,128]{3,1,2,0:T(8,128)(2,1)} fusion(bf16[8,512,1,128]{3,1,2,0:T(8,128)(2,1)} %get-tuple-element.141, s32[]{:T(128)} %get-tuple-element.140, f32[512,4096]{1,0:T(8,128)S(1)} %get-tuple-element.130, f32[512]{0:T(512)S(1)} %fusion.47, f32[512]{0:T(512)S(1)} %get-tuple-element.131, bf16[4096,1,128]{2,0,1:T(8,128)(2,1)S(1)} %copy-done.1), kind=kOutput, calls=%fused_computation.10.clone.1 | convolution fusion | flops 543227904 | bytes 9572864 | tf_op jit(solution)/shard_map/while/body/eval_jaxpr/hqk,khd->qhd/dot_general | solution.py:110
  183.9 2.0 fusion.46
  185.9 1.3 fusion.47
  187.2 2.8 %fusion.48 = bf16[8,512,1,128]{3,1,2,0:T(8,128)(2,1)} fusion(bf16[8,512,1,128]{3,1,2,0:T(8,128)(2,1)} %get-tuple-element.141, s32[]{:T(128)} %get-tuple-element.140, f32[512,4096]{1,0:T(8,128)S(1)} %get-tuple-element.130, f32[512]{0:T(512)S(1)} %fusion.47, f32[512]{0:T(512)S(1)} %get-tuple-element.131, bf16[4096,1,128]{2,0,1:T(8,128)(2,1)S(1)} %copy-done.1), kind=kOutput, calls=%fused_computation.10.clone.1 | convolution fusion | flops 543227904 | bytes 9572864 | tf_op jit(solution)/shard_map/while/body/eval_jaxpr/hqk,khd->qhd/dot_general | solution.py:110
  191.3 2.0 fusion.46
  193.3 1.3 fusion.47
  194.6 2.8 %fusion.48 = bf16[8,512,1,128]{3,1,2,0:T(8,128)(2,1)} fusion(bf16[8,512,1,128]{3,1,2,0:T(8,128)(2,1)} %get-tuple-element.141, s32[]{:T(128)} %get-tuple-element.140, f32[512,4096]{1,0:T(8,128)S(1)} %get-tuple-element.130, f32[512]{0:T(512)S(1)} %fusion.47, f32[512]{0:T(512)S(1)} %get-tuple-element.131, bf16[4096,1,128]{2,0,1:T(8,128)(2,1)S(1)} %copy-done.1), kind=kOutput, calls=%fused_computation.10.clone.1 | convolution fusion | flops 543227904 | bytes 9572864 | tf_op jit(solution)/shard_map/while/body/eval_jaxpr/hqk,khd->qhd/dot_general | solution.py:110
  197.4 21.8 %all_to_all.23 = bf16[16,256,128]{2,1,0:T(8,128)(2,1)S(1)} all-to-all(bf16[16,256,128]{2,1,0:T(8,128)(2,1)} %bitcast.8), channel_id=1, replica_groups=mesh['sp'=16,'dp'=8] {'sp'}, dimensions={0} | all-to-all | bytes 2097152 | tf_op jit(solution)/shard_map/all_to_all | solution.py:163
  219.2 1.6 convert_bitcast_fusion
  220.8 1.9 copy.42
  223.4 6.7 %fusion.15 = bf16[1,256,2048]{2,1,0:T(8,128)(2,1)} fusion(bf16[256,2048]{0,1:T(8,128)(2,1)S(1)} %fusion.23, bf16[2048,2048]{1,0:T(8,128)(2,1)} %all-gather.8.cloned.1.call-done), kind=kOutput, calls=%fused_computation.31 | convolution fusion | flops 2148007936 | bytes 10485760 | tf_op jit(solution)/shard_map/dot_general | solution.py:81
  (85 shorter events, 10.0 us)
Async XLA Ops:
  6.5 3.5 %copy-start = (bf16[2048,64]{0,1:T(8,128)(2,1)S(1)}, bf16[2048,64]{0,1:T(8,128)(2,1)}, u32[]{:S(2)}) copy-start(bf16[2048,64]{0,1:T(8,128)(2,1)} %param.20) | copy-start | bytes 786436
  6.5 32.7 %copy-start.2 = (bf16[1,256,2048]{2,1,0:T(8,128)(2,1)S(1)}, bf16[1,256,2048]{2,1,0:T(8,128)(2,1)}, u32[]{:S(2)}) copy-start(bf16[1,256,2048]{2,1,0:T(8,128)(2,1)} %param.16) | copy-start | bytes 3145732
  6.5 32.7 %copy-start.10 = (f32[2048]{0:T(1024)S(1)}, f32[2048]{0:T(1024)}, u32[]{:S(2)}) copy-start(f32[2048]{0:T(1024)} %param.17) | copy-start | bytes 24580
  6.5 32.7 %all-gather.4.cloned.1.call-start = ((), (), s32[]{:S(2)}) async-start(), calls=%async_computation.3 | async-start | bytes 3538944 | tf_op jit(solution)/shard_map/all_gather | solution.py:18
  8.5 102.7 %all-gather.6.cloned.1.call-start = ((), (), s32[]{:S(2)}) async-start(), calls=%async_computation.4 | async-start | bytes 7798784 | tf_op jit(solution)/shard_map/all_gather | solution.py:18
  41.6 2.1 copy-start.6
  41.6 2.2 copy-start.7
  41.7 3.2 %copy-start.4 = (bf16[32,128]{1,0:T(8,128)(2,1)S(1)}, bf16[32,128]{1,0:T(8,128)(2,1)}, u32[]{:S(2)}) copy-start(bf16[32,128]{1,0:T(8,128)(2,1)} %param.24) | copy-start | bytes 24580
  41.7 7.9 %copy-start.5 = (bf16[32,128]{1,0:T(8,128)(2,1)S(1)}, bf16[32,128]{1,0:T(8,128)(2,1)}, u32[]{:S(2)}) copy-start(bf16[32,128]{1,0:T(8,128)(2,1)} %param.25) | copy-start | bytes 24580
  45.5 67.7 %all-to-all-start.1 = ((bf16[8,32,128]{2,1,0:T(8,128)(2,1)}), bf16[8,32,128]{2,1,0:T(8,128)(2,1)S(1)}, u32[]{:S(2)}, u32[]{:S(2)}) async-start(bf16[8,32,128]{2,1,0:T(8,128)(2,1)} %stack.2), calls=%async_computation.1 | async-start | bytes 131072 | tf_op jit(solution)/shard_map/all_to_all | solution.py:154
  48.8 174.6 %all-gather.8.cloned.1.call-start = ((), (), s32[]{:S(2)}) async-start(), calls=%async_computation.5 | async-start | bytes 8454144 | tf_op jit(solution)/shard_map/all_gather | solution.py:165
  114.6 11.9 %all-to-all-start = ((bf16[8,64,192]{2,1,0:T(8,128)(2,1)}), bf16[8,64,192]{2,1,0:T(8,128)(2,1)}, u32[]{:S(2)}, u32[]{:S(2)}) async-start(bf16[8,64,192]{2,1,0:T(8,128)(2,1)} %broadcast_in_dim.11), calls=%async_computation | async-start | bytes 524288 | tf_op jit(solution)/shard_map/all_to_all | solution.py:29
  126.5 3.8 %copy-start.8 = (f32[192]{0:T(256)S(1)}, f32[192]{0:T(256)}, u32[]{:S(2)}) copy-start(f32[192]{0:T(256)} %param.27) | copy-start | bytes 2308
  130.3 0.7 copy-start.9
  141.1 1.3 copy-start.1
  148.5 1.3 copy-start.1
  155.9 1.3 copy-start.1
  163.3 1.5 copy-start.1
  171.0 1.4 copy-start.1
  178.5 1.3 copy-start.1
  185.9 1.3 copy-start.1
  193.3 1.3 copy-start.1
  220.8 2.2 copy-start.3
Sparse Core Ops, SparseCore 0:
  9.0 30.1 all-gather.3
  44.9 66.1 all-gather.5
  114.2 69.3 all-gather.7
